TPU v7x, 32 devices: a whole 2x2x4 slice. The times are simulated.
32 devices in a mesh: fs: 4 (over y, x), tp: 8 (over z, core).
Axes of the slice: x: 2, y: 2, z: 4, core: 2. Of those that a mesh axis runs over, the one named last changes fastest.
Arguments:
- tokens: bfloat16 [4096, 2048], P(('fs', 'tp')), may hold values from -6 to 6
- norm_gain: float32 [2048], replicated, may hold values from 0.1 to 1.9
- gate_weight: bfloat16 [2048, 5632], P('fs', 'tp'), may hold values from -0.125 to 0.125
- up_weight: bfloat16 [2048, 5632], P('fs', 'tp'), may hold values from -0.125 to 0.125
- down_weight: bfloat16 [5632, 2048], P('tp', 'fs'), may hold values from -0.078125 to 0.078125
Outputs:
- mixed: bfloat16 [4096, 2048], P(('fs', 'tp'))
All inputs are finite; a program needn't handle non-finite values.
Results may differ from a plain program's by a relative error of at most 0.0065.
Values may be sent and summed in bfloat16 or wider, within the bound.
A program may use at most 128 MiB of HBM per device.

v0:
```python
import jax
import jax.numpy as jnp
from jax import lax
from jax.sharding import PartitionSpec as P

eps_floor = 0.05


def local(tokens, norm_gain, gate_weight, up_weight, down_weight):
    values = tokens.astype(jnp.float32)
    factor = lax.rsqrt(jnp.mean(values * values, axis=-1, keepdims=True) + eps_floor)
    normed = (values * factor * norm_gain).astype(jnp.bfloat16)
    local_ff = gate_weight.shape[1]
    group = lax.all_gather(normed, "tp", axis=0, tiled=True)
    joined = jnp.concatenate(
        (
            lax.all_gather(gate_weight, "fs", axis=0, tiled=True),
            lax.all_gather(up_weight, "fs", axis=0, tiled=True),
        ),
        axis=1,
    )
    product = jnp.dot(group, joined, preferred_element_type=jnp.float32)
    hidden = (jax.nn.silu(product[:, :local_ff]) * product[:, local_ff:]).astype(jnp.bfloat16)
    down_local = lax.all_gather(down_weight, "fs", axis=1, tiled=True)
    mixed = lax.psum_scatter(
        jnp.dot(hidden, down_local, preferred_element_type=jnp.float32),
        "tp",
        scatter_dimension=0,
        tiled=True,
    )
    return mixed.astype(jnp.bfloat16)


def solution(mesh):
    return jax.shard_map(
        local,
        mesh=mesh,
        in_specs=(P(("fs", "tp"), None), P(), P("fs", "tp"), P("fs", "tp"), P("tp", "fs")),
        out_specs=P(("fs", "tp"), None),
        check_vma=False,
    )
```

profile of v0, /device:TPU:0, one launch (start us, length us, event | category | flops | bytes accessed | tf_op | source)
XLA Modules:
  0.0 296.1 jit_solution(4076748041551358290)
XLA Ops:
  6.5 0.0 all-gather.7.cloned.1.call-start
  6.5 0.7 all-gather.7.cloned.1.call-update
  7.3 0.0 all-gather.9.cloned.1.call-start
  7.3 0.7 all-gather.9.cloned.1.call-update
  8.0 0.0 all-gather.5.cloned.1.call-start
  8.1 1.2 fusion.8
  9.3 2.0 fusion.10
  11.3 0.0 all-gather.5.cloned.1.call-update
  11.3 0.0 all-gather.11.cloned.1.call-start
  11.4 0.5 all-gather.11.cloned.1.call-update
  11.9 0.0 reduce-scatter.2.cloned.1.call-start
  12.0 41.5 %all-gather.7.cloned.1.call-done = bf16[2048,704]{0,1:T(8,128)(2,1)} async-done(((bf16[512,704]{0,1:T(8,128)(2,1)}), bf16[2048,704]{0,1:T(8,128)(2,1)}) %all-gather.7.cloned.1.call-update) | async-done | bytes 2883600 | tf_op jit(solution)/shard_map/all_gather | solution.py:17
  53.5 43.4 %all-gather.9.cloned.1.call-done = bf16[2048,704]{0,1:T(8,128)(2,1)} async-done(((bf16[512,704]{0,1:T(8,128)(2,1)}), bf16[2048,704]{0,1:T(8,128)(2,1)}) %all-gather.9.cloned.1.call-update) | async-done | bytes 2883600 | tf_op jit(solution)/shard_map/all_gather | solution.py:18
  96.9 48.5 %all-gather.5.cloned.1.call-done = bf16[1024,2048]{1,0:T(8,128)(2,1)} async-done(((bf16[128,2048]{1,0:T(8,128)(2,1)}), bf16[1024,2048]{1,0:T(8,128)(2,1)}) %all-gather.5.cloned.1.call-update) | async-done | bytes 4194320 | tf_op jit(solution)/shard_map/all_gather | solution.py:14
  145.4 11.8 %fusion = f32[1024,1408]{1,0:T(8,128)} fusion(bf16[1024,2048]{1,0:T(8,128)(2,1)} %all-gather.5.cloned.1.call-done, bf16[2048,704]{0,1:T(8,128)(2,1)} %all-gather.9.cloned.1.call-done, bf16[2048,704]{0,1:T(8,128)(2,1)} %all-gather.7.cloned.1.call-done), kind=kOutput, calls=%fused_computation | convolution fusion | flops 5917114368 | bytes 15728640 | tf_op jit(solution)/shard_map/dot_general | solution.py:22
  157.2 30.2 %all-gather.11.cloned.1.call-done = bf16[704,2048]{1,0:T(8,128)(2,1)} async-done(((bf16[704,512]{1,0:T(8,128)(2,1)}), bf16[704,2048]{1,0:T(8,128)(2,1)}) %all-gather.11.cloned.1.call-update) | async-done | bytes 2883600 | tf_op jit(solution)/shard_map/all_gather | solution.py:24
  187.4 10.4 %fusion.5 = f32[1024,2048]{1,0:T(8,128)} fusion(bf16[704,2048]{1,0:T(8,128)(2,1)} %all-gather.11.cloned.1.call-done, f32[1024,1408]{1,0:T(8,128)} %fusion), kind=kOutput, calls=%fused_computation.6 | convolution fusion | flops 2957115392 | bytes 17563648 | tf_op jit(solution)/shard_map/dot_general | solution.py:26
  197.8 0.0 reduce-scatter.2.cloned.1.call-update
  197.8 89.7 %reduce-scatter.2.cloned.1.call-done = f32[128,2048]{1,0:T(8,128)} async-done(((f32[1024,2048]{1,0:T(8,128)}), f32[128,2048]{1,0:T(8,128)}) %reduce-scatter.2.cloned.1.call-update) | async-done | bytes 1048592 | tf_op jit(solution)/shard_map/reduce_scatter | solution.py:25
  287.5 2.1 convert_element_type.15
  (1 shorter events, 0.0 us)
Async XLA Ops:
  6.5 46.9 %all-gather.7.cloned.1.call-start = ((), (), s32[]{:S(2)}) async-start(), calls=%async_computation.2 | async-start | bytes 3604480 | tf_op jit(solution)/shard_map/all_gather | solution.py:17
  7.3 89.6 %all-gather.9.cloned.1.call-start = ((), (), s32[]{:S(2)}) async-start(), calls=%async_computation.3 | async-start | bytes 3604480 | tf_op jit(solution)/shard_map/all_gather | solution.py:18
  8.0 137.3 %all-gather.5.cloned.1.call-start = ((), (), s32[]{:S(2)}) async-start(), calls=%async_computation.1 | async-start | bytes 4718592 | tf_op jit(solution)/shard_map/all_gather | solution.py:14
  11.3 176.1 %all-gather.11.cloned.1.call-start = ((), (), s32[]{:S(2)}) async-start(), calls=%async_computation.4 | async-start | bytes 3604480 | tf_op jit(solution)/shard_map/all_gather | solution.py:24
  11.9 275.6 %reduce-scatter.2.cloned.1.call-start = ((), (), s32[]{:S(2)}) async-start(), calls=%async_computation.5 | async-start | bytes 9437184 | tf_op jit(solution)/shard_map/reduce_scatter | solution.py:25
Sparse Core Ops, SparseCore 0:
  9.2 44.2 all-gather.6
  55.3 41.5 all-gather.8
  98.5 46.8 all-gather.4
  147.0 40.3 all-gather.10
  198.0 89.5 reduce-scatter.1
where the time goes:
time: 296 us
  waiting for transfers between devices  255 us (86%)
  matrix products  22.2 us (8%)
  between operations  13.1 us (4%)
  other arithmetic  5.35 us (2%)
    reduce_scatter x1, waiting for transfers between devices, local(): lax.psum_scatter(jnp.dot(hidden, down_local, preferred_element_type=jnp.f...  89.7 us
    all_gather x1, waiting for transfers between devices, local(): group = lax.all_gather(normed, 'tp', axis=0, tiled=True)  48.5 us
    all_gather x1, waiting for transfers between devices, local(): lax.all_gather(up_weight, 'fs', axis=0, tiled=True)  43.4 us
    all_gather x1, waiting for transfers between devices, local(): lax.all_gather(gate_weight, 'fs', axis=0, tiled=True)  41.5 us
    all_gather x1, waiting for transfers between devices, local(): down_local = lax.all_gather(down_weight, 'fs', axis=1, tiled=True)  30.2 us
    dot_general x1, matrix products, local(): product = jnp.dot(group, joined, preferred_element_type=jnp.float32)  11.8 us
    dot_general x1, matrix products, local(): jnp.dot(hidden, down_local, preferred_element_type=jnp.float32)  10.4 us
  transfers between devices with their start and end apart: 5, of which 5 were waited for; matrix products, arithmetic and copies ran while one was open for 5% of the time, Pallas kernels for 0%

commit v1 on v0

--- a/solution.py
+++ b/solution.py
@@ -21,7 +21,8 @@
     )
     product = jnp.dot(group, joined, preferred_element_type=jnp.float32)
     hidden = (jax.nn.silu(product[:, :local_ff]) * product[:, local_ff:]).astype(jnp.bfloat16)
-    down_local = lax.all_gather(down_weight, "fs", axis=1, tiled=True)
+    sent = jnp.stack([down_weight] * lax.axis_size("fs"))
+    down_local = jnp.concatenate(lax.all_to_all(sent, "fs", 0, 0), axis=1)
     mixed = lax.psum_scatter(
         jnp.dot(hidden, down_local, preferred_element_type=jnp.float32),
         "tp",

time: 296 us -> 279 us (0.943)
  waiting for transfers between devices: 255 us -> 192 us
  blocking collectives: 0 us -> 51.5 us
  matrix products: 22.2 us -> 16.6 us
    all_to_all x0 -> x1, blocking collectives: none -> 51.5 us  [local(): down_local = jnp.concatenate(lax.all_to_all(sent, 'fs', 0, 0), axis=1)]
    all_gather x1, waiting for transfers between devices: 41.5 us -> 9.73 us  [local(): lax.all_gather(gate_weight, 'fs', axis=0, tiled=True)]
    all_gather x1 -> x0, waiting for transfers between devices: 30.2 us -> none  [local(): down_local = lax.all_gather(down_weight, 'fs', axis=1, tiled=True)]
    dot_general x1, matrix products: 10.4 us -> 5.83 us  [local(): jnp.dot(hidden, down_local, preferred_element_type=jnp.float32)]
  transfers between devices with their start and end apart: 5 -> 4, of which waited for: 5 -> 4; matrix products, arithmetic and copies ran while one was open for 5% -> 1% of each run, Pallas kernels for 0% -> 0%
where the time goes in v1:
time: 279 us
  waiting for transfers between devices  192 us (69%)
  blocking collectives  51.5 us (18%)
  matrix products  16.6 us (6%)
  between operations  13.2 us (5%)
  other arithmetic  5.35 us (2%)
    reduce_scatter x1, waiting for transfers between devices, local(): lax.psum_scatter(jnp.dot(hidden, down_local, preferred_element_type=jnp.f...  88.5 us
    all_to_all x1, blocking collectives, local(): down_local = jnp.concatenate(lax.all_to_all(sent, 'fs', 0, 0), axis=1)  51.5 us
    all_gather x1, waiting for transfers between devices, local(): group = lax.all_gather(normed, 'tp', axis=0, tiled=True)  48.5 us
    all_gather x1, waiting for transfers between devices, local(): lax.all_gather(up_weight, 'fs', axis=0, tiled=True)  43.7 us
    dot_general x1, matrix products, local(): product = jnp.dot(group, joined, preferred_element_type=jnp.float32)  10.8 us
    all_gather x1, waiting for transfers between devices, local(): lax.all_gather(gate_weight, 'fs', axis=0, tiled=True)  9.73 us
    dot_general x1, matrix products, local(): jnp.dot(hidden, down_local, preferred_element_type=jnp.float32)  5.83 us
  transfers between devices with their start and end apart: 4, of which 4 were waited for; matrix products, arithmetic and copies ran while one was open for 1% of the time, Pallas kernels for 0%

profile of v1, /device:TPU:0, one launch (start us, length us, event | category | flops | bytes accessed | tf_op | source)
XLA Modules:
  0.0 279.2 jit_solution(14670812214996396466)
XLA Ops:
  6.5 0.0 copy-start
  6.5 0.0 all-gather.6.cloned.1.call-start
  6.5 0.7 all-gather.6.cloned.1.call-update
  7.3 0.0 all-gather.8.cloned.1.call-start
  7.3 0.7 all-gather.8.cloned.1.call-update
  8.0 0.0 all-gather.4.cloned.1.call-start
  8.1 1.2 fusion.8
  9.3 2.0 fusion.10
  11.3 0.0 all-gather.4.cloned.1.call-update
  11.3 0.0 reduce-scatter.2.cloned.1.call-start
  11.4 0.0 copy-done
  11.4 0.2 stack.2
  11.6 51.5 %all_to_all.5 = bf16[4,704,512]{2,1,0:T(8,128)(2,1)S(1)} all-to-all(bf16[4,704,512]{2,1,0:T(8,128)(2,1)S(1)} %stack.2), channel_id=1, replica_groups=mesh['fs'=4,'tp'=8] {'fs'}, dimensions={0} | all-to-all | bytes 5767168 | tf_op jit(solution)/shard_map/all_to_all | solution.py:25
  63.1 0.4 copy.7
  63.6 9.7 %all-gather.6.cloned.1.call-done = bf16[2048,704]{0,1:T(8,128)(2,1)} async-done(((bf16[512,704]{0,1:T(8,128)(2,1)}), bf16[2048,704]{0,1:T(8,128)(2,1)}) %all-gather.6.cloned.1.call-update) | async-done | bytes 2883600 | tf_op jit(solution)/shard_map/all_gather | solution.py:17
  73.3 43.7 %all-gather.8.cloned.1.call-done = bf16[2048,704]{0,1:T(8,128)(2,1)} async-done(((bf16[512,704]{0,1:T(8,128)(2,1)}), bf16[2048,704]{0,1:T(8,128)(2,1)}) %all-gather.8.cloned.1.call-update) | async-done | bytes 2883600 | tf_op jit(solution)/shard_map/all_gather | solution.py:18
  117.0 48.5 %all-gather.4.cloned.1.call-done = bf16[1024,2048]{1,0:T(8,128)(2,1)} async-done(((bf16[128,2048]{1,0:T(8,128)(2,1)}), bf16[1024,2048]{1,0:T(8,128)(2,1)}) %all-gather.4.cloned.1.call-update) | async-done | bytes 4194320 | tf_op jit(solution)/shard_map/all_gather | solution.py:14
  165.5 10.8 %fusion = f32[1024,1408]{1,0:T(8,128)S(1)} fusion(bf16[1024,2048]{1,0:T(8,128)(2,1)} %all-gather.4.cloned.1.call-done, bf16[2048,704]{0,1:T(8,128)(2,1)} %all-gather.8.cloned.1.call-done, bf16[2048,704]{0,1:T(8,128)(2,1)} %all-gather.6.cloned.1.call-done), kind=kOutput, calls=%fused_computation | convolution fusion | flops 5917114368 | bytes 15728640 | tf_op jit(solution)/shard_map/dot_general | solution.py:22
  176.2 5.8 %fusion.5 = f32[1024,2048]{1,0:T(8,128)} fusion(bf16[704,2048]{1,0:T(8,128)(2,1)S(1)} %bitcast.6, f32[1024,1408]{1,0:T(8,128)S(1)} %fusion), kind=kOutput, calls=%fused_computation.6 | convolution fusion | flops 2957115392 | bytes 17563648 | tf_op jit(solution)/shard_map/dot_general | solution.py:27
  182.1 0.0 reduce-scatter.2.cloned.1.call-update
  182.1 88.5 %reduce-scatter.2.cloned.1.call-done = f32[128,2048]{1,0:T(8,128)} async-done(((f32[1024,2048]{1,0:T(8,128)}), f32[128,2048]{1,0:T(8,128)}) %reduce-scatter.2.cloned.1.call-update) | async-done | bytes 1048592 | tf_op jit(solution)/shard_map/reduce_scatter | solution.py:26
  270.6 2.1 convert_element_type.15
  (1 shorter events, 0.0 us)
Async XLA Ops:
  6.5 4.9 %copy-start = (bf16[704,512]{1,0:T(8,128)(2,1)S(1)}, bf16[704,512]{1,0:T(8,128)(2,1)}, u32[]{:S(2)}) copy-start(bf16[704,512]{1,0:T(8,128)(2,1)} %param.9) | copy-start | bytes 2162692
  6.5 66.8 %all-gather.6.cloned.1.call-start = ((), (), s32[]{:S(2)}) async-start(), calls=%async_computation.3 | async-start | bytes 3604480 | tf_op jit(solution)/shard_map/all_gather | solution.py:17
  7.3 109.7 %all-gather.8.cloned.1.call-start = ((), (), s32[]{:S(2)}) async-start(), calls=%async_computation.4 | async-start | bytes 3604480 | tf_op jit(solution)/shard_map/all_gather | solution.py:18
  8.0 157.5 %all-gather.4.cloned.1.call-start = ((), (), s32[]{:S(2)}) async-start(), calls=%async_computation.2 | async-start | bytes 4718592 | tf_op jit(solution)/shard_map/all_gather | solution.py:14
  11.3 259.2 %reduce-scatter.2.cloned.1.call-start = ((), (), s32[]{:S(2)}) async-start(), calls=%async_computation.5 | async-start | bytes 9437184 | tf_op jit(solution)/shard_map/reduce_scatter | solution.py:26
Sparse Core Ops, SparseCore 0:
  9.2 64.1 all-gather.5
  75.1 41.7 all-gather.7
  118.6 46.8 all-gather.3
  182.2 88.3 reduce-scatter.1
